TPU v7x, 32 devices: a whole 2x2x4 slice. The times are simulated.
32 devices in a mesh: sp: 8 (over z, x), tp: 4 (over y, core).
Axes of the slice: x: 2, y: 2, z: 4, core: 2. Of those that a mesh axis runs over, the one named last changes fastest.
Arguments:
- tokens: bfloat16 [1024, 2048], P(('sp', 'tp')), may hold values from -6 to 6
- input_norm_gain: float32 [2048], replicated, may hold values from 0.1 to 1.9
- convolution_value_weight: bfloat16 [2048, 1024], P('sp', 'tp'), may hold values from -0.125 to 0.125
- convolution_gate_weight: bfloat16 [2048, 1024], P('sp', 'tp'), may hold values from -0.125 to 0.125
- depthwise_filter_taps: float32 [31, 1024], P(None, 'tp'), may hold values from -4 to 4
- channel_norm_gain: float32 [1024], P('tp'), may hold values from 0.1 to 1.9
- channel_norm_bias: float32 [1024], P('tp'), may hold values from -3 to 3
- query_projection_weight: bfloat16 [2048, 1024], P('sp', 'tp'), may hold values from -0.125 to 0.125
- forget_gate_weight: bfloat16 [2048, 1024], P('sp', 'tp'), may hold values from -0.125 to 0.125
- recurrence_value_weight: bfloat16 [2048, 1024], P('sp', 'tp'), may hold values from -0.125 to 0.125
- output_gate_weight: bfloat16 [2048, 1024], P('sp', 'tp'), may hold values from -0.125 to 0.125
- forget_floor_margin: float32 [1024], P('tp'), may hold values from 9.765625e-05 to 0.1
- decay_jump_terms: float32 [8, 1024], P('tp', 'sp'), may hold values from -0.7 to 0
- head_norm_gain: float32 [1024], P('tp'), may hold values from 0.1 to 1.9
- convolution_output_weight: bfloat16 [1024, 2048], P('tp', 'sp'), may hold values from -0.125 to 0.125
- recurrence_output_weight: bfloat16 [1024, 2048], P('tp', 'sp'), may hold values from -0.125 to 0.125
Outputs:
- mixed: bfloat16 [1024, 2048], P(('sp', 'tp'))
All inputs are finite; a program needn't handle non-finite values.
Results may differ from a plain program's by a relative error of at most 0.015.
Values may be sent and summed in bfloat16 or wider, within the bound.
A program may use at most 64 MiB of HBM per device.

v0:
```python
import jax
import jax.numpy as jnp
from jax import lax
from jax.sharding import PartitionSpec as P

CONV_CH = 1024
HG_DK = 128
HG_DV = 128
HG_BLOCK = 64
norm_eps = 1e-06
layer_eps = 1e-05
highest_precision = lax.Precision.HIGHEST


def passed_along(value, axis, steps):
    count = lax.axis_size(axis)
    initial, last = (max(0, -steps), min(count, count - steps))
    return lax.ppermute(value, axis, [(source, source + steps) for source in range(initial, last)])


def prefix(x, axis, combine, identity):
    size, mine = (lax.axis_size(axis), lax.axis_index(axis))
    everything = jax.tree.map(
        lambda part, kind: lax.all_gather(part.astype(kind), axis), x, (jnp.bfloat16, jnp.bfloat16)
    )
    start = jax.tree.map(
        lambda part, zero: jnp.broadcast_to(jnp.asarray(zero, part.dtype), part.shape), x, identity
    )

    def lap(k, before):
        reached = k < mine
        new = combine(
            before, jax.tree.map(lambda part, own: part[k].astype(own.dtype), everything, x)
        )
        return jax.tree.map(lambda a, b: jnp.where(reached, a, b), new, before)

    return lax.fori_loop(0, size, lap, start)


def convolve(gated, kernel):
    return lax.conv_general_dilated(
        gated[None],
        kernel[:, None, :],
        (1,),
        "VALID",
        dimension_numbers=("NWC", "WIO", "NWC"),
        feature_group_count=gated.shape[1],
        precision=highest_precision,
    )[0]


def channel_norm(values, first_sum, second_sum, gain, bias):
    mean_value = first_sum[:, None] / CONV_CH
    variance = second_sum[:, None] / CONV_CH - mean_value * mean_value
    shifted = (values - mean_value) * lax.rsqrt(variance + layer_eps) * gain + bias
    return jax.nn.silu(shifted).astype(jnp.bfloat16)


def gate_factors(query_projected, forget_projected, forget_floor_margin, decay_jump_rows):
    row_total_count = query_projected.shape[0]
    head_total_count = decay_jump_rows.shape[1]
    query_rows = jax.nn.silu(query_projected.astype(jnp.float32))
    log_forget_gate = jnp.logaddexp(
        jnp.log1p(-forget_floor_margin),
        jnp.log(forget_floor_margin) + jax.nn.log_sigmoid(forget_projected.astype(jnp.float32)),
    )
    key_gate_values = -jnp.expm1(log_forget_gate)
    log_decay_running = (
        log_forget_gate.reshape(row_total_count, head_total_count, -1) + decay_jump_rows[:, :, None]
    )
    return (
        query_rows.reshape(row_total_count, head_total_count, -1),
        key_gate_values.reshape(row_total_count, head_total_count, -1),
        log_decay_running,
    )


def finish(recurrent, gain, outgate_proj):
    row_total_count = recurrent.shape[0]
    scaled = recurrent * lax.rsqrt(
        jnp.mean(recurrent * recurrent, axis=2, keepdims=True) + norm_eps
    )
    gated_out = (
        scaled.reshape(row_total_count, -1) * gain * jax.nn.silu(outgate_proj.astype(jnp.float32))
    )
    return gated_out.astype(jnp.bfloat16)


def combine_states(first_part, second_part):
    return (
        first_part[0] + second_part[0],
        jnp.exp(second_part[0])[:, :, None] * first_part[1] + second_part[1],
    )


def carry_step(recurrence_state, block_parts):
    decay_end, contribution = block_parts
    return (jnp.exp(decay_end)[:, :, None] * recurrence_state + contribution, recurrence_state)


def per_device(
    tokens,
    input_norm_gain,
    convolution_value_weight,
    convolution_gate_weight,
    depthwise_filter_taps,
    channel_norm_gain,
    channel_norm_bias,
    query_projection_weight,
    forget_gate_weight,
    recurrence_value_weight,
    output_gate_weight,
    forget_floor_margin,
    decay_jump_terms,
    head_norm_gain,
    convolution_output_weight,
    recurrence_output_weight,
):
    features = tokens.astype(jnp.float32)
    normed = (
        features
        * lax.rsqrt(jnp.mean(features * features, axis=1, keepdims=True) + norm_eps)
        * input_norm_gain
    ).astype(jnp.bfloat16)
    gathered = (
        lax.all_gather(convolution_value_weight, "sp", axis=0, tiled=True),
        lax.all_gather(convolution_gate_weight, "sp", axis=0, tiled=True),
        lax.all_gather(query_projection_weight, "sp", axis=0, tiled=True),
        lax.all_gather(forget_gate_weight, "sp", axis=0, tiled=True),
        lax.all_gather(recurrence_value_weight, "sp", axis=0, tiled=True),
        lax.all_gather(output_gate_weight, "sp", axis=0, tiled=True),
        lax.all_gather(convolution_output_weight, "sp", axis=1, tiled=True),
        lax.all_gather(recurrence_output_weight, "sp", axis=1, tiled=True),
    )
    projection_weights = gathered[:6]
    conv_columns = gathered[6]
    rec_columns = gathered[7]

    def project(row_piece):
        return jnp.concatenate(
            [
                jnp.dot(row_piece, weight, preferred_element_type=jnp.float32).astype(jnp.bfloat16)
                for weight in projection_weights
            ],
            axis=1,
        )

    projected = project(lax.all_gather(normed, "tp", axis=0, tiled=True))
    offsets = []
    position = 0
    for weight in projection_weights[:-1]:
        position = position + weight.shape[1]
        offsets.append(position)
    value_proj, gate_proj, query_projected, forget_projected, input_proj, outgate_proj = jnp.split(
        projected, offsets, axis=1
    )
    row_total_count = value_proj.shape[0]
    rim_rows = depthwise_filter_taps.shape[0] - 1
    tail_value, tail_gate = passed_along(
        (value_proj[row_total_count - rim_rows :], gate_proj[row_total_count - rim_rows :]), "sp", 1
    )
    value_ext = jnp.concatenate([tail_value, value_proj], axis=0)
    gate_ext = jnp.concatenate([tail_gate, gate_proj], axis=0)
    gated = value_ext.astype(jnp.float32) * jax.nn.sigmoid(gate_ext.astype(jnp.float32))
    convolved = convolve(gated, depthwise_filter_taps).astype(jnp.bfloat16)
    device_heads = decay_jump_terms.shape[0]
    query_rows, key_gate_values, log_decay_running = gate_factors(
        query_projected, forget_projected, forget_floor_margin, decay_jump_terms.T
    )
    input_rows = input_proj.astype(jnp.float32).reshape(row_total_count, device_heads, -1)
    block_count = row_total_count // HG_BLOCK

    def to_blocks(array):
        return array.reshape(block_count, HG_BLOCK, device_heads, -1).transpose(0, 2, 1, 3)

    block_queries = to_blocks(query_rows)
    block_keys = to_blocks(key_gate_values)
    block_inputs = to_blocks(input_rows)
    cumulative = jnp.cumsum(to_blocks(log_decay_running), axis=2)
    final_decay = cumulative[:, :, -1, :]
    query_rows_scaled = block_queries * jnp.exp(cumulative)
    scaled_keys = block_keys * jnp.exp(-cumulative)
    final_keys = block_keys * jnp.exp(final_decay[:, :, None, :] - cumulative)
    attention_scores = jnp.einsum(
        "nhtk,nhsk->nhts", query_rows_scaled, scaled_keys, precision=highest_precision
    )
    causal = jnp.arange(HG_BLOCK)[:, None] >= jnp.arange(HG_BLOCK)[None, :]
    attention_scores = jnp.where(causal[None, None], attention_scores, 0.0)
    inner = jnp.einsum(
        "nhts,nhsv->nhtv", attention_scores, block_inputs, precision=highest_precision
    )
    contributions = jnp.einsum(
        "nhsk,nhsv->nhkv", final_keys, block_inputs, precision=highest_precision
    )
    initial = jnp.zeros((device_heads, HG_DK, HG_DV), jnp.float32)
    local_state, block_starts = lax.scan(carry_step, initial, (final_decay, contributions))
    device_decay = jnp.sum(final_decay, axis=0)
    before_blocks = jnp.cumsum(final_decay, axis=0) - final_decay
    incoming = prefix(
        (device_decay, local_state),
        "sp",
        combine_states,
        (jnp.zeros_like(device_decay), jnp.zeros_like(local_state)),
    )
    starts = block_starts + jnp.exp(before_blocks)[:, :, :, None] * incoming[1][None]
    recurrent = inner + jnp.einsum(
        "nhtk,nhkv->nhtv", query_rows_scaled, starts, precision=highest_precision
    )
    recurrent = recurrent.transpose(0, 2, 1, 3).reshape(row_total_count, device_heads, -1)
    rec_out = finish(recurrent, head_norm_gain, outgate_proj)
    values = convolved.astype(jnp.float32)
    totals = lax.psum((jnp.sum(values, axis=1), jnp.sum(values * values, axis=1)), "tp")
    conv_out = channel_norm(values, totals[0], totals[1], channel_norm_gain, channel_norm_bias)
    conv_part = lax.slice_in_dim(
        conv_out, 0, row_total_count // lax.axis_size("tp") * lax.axis_size("tp"), axis=0
    )
    return lax.psum_scatter(
        (
            jnp.dot(conv_part, conv_columns, preferred_element_type=jnp.float32)
            + jnp.dot(rec_out, rec_columns, preferred_element_type=jnp.float32)
        ).astype(jnp.bfloat16),
        "tp",
        scatter_dimension=0,
        tiled=True,
    )


def solution(mesh):
    in_specs = (
        P(("sp", "tp"), None),
        P(),
        P("sp", "tp"),
        P("sp", "tp"),
        P(None, "tp"),
        P("tp"),
        P("tp"),
        P("sp", "tp"),
        P("sp", "tp"),
        P("sp", "tp"),
        P("sp", "tp"),
        P("tp"),
        P("tp", "sp"),
        P("tp"),
        P("tp", "sp"),
        P("tp", "sp"),
    )
    out_specs = P(("sp", "tp"), None)
    return jax.shard_map(
        per_device, mesh=mesh, in_specs=in_specs, out_specs=out_specs, check_vma=False
    )
```

profile of v0, /device:TPU:0, one launch (start us, length us, event | category | flops | bytes accessed | tf_op | source)
XLA Modules:
  0.0 371.7 jit_solution(17329059093912126885)
XLA Ops:
  6.5 0.7 all-gather.20.cloned.1.call-update
  7.3 0.7 all-gather.22.cloned.1.call-update
  8.1 0.7 all-gather.18.cloned.1.call-update
  8.8 0.5 all-gather.12.cloned.1.call-update
  9.4 0.5 all-gather.14.cloned.1.call-update
  10.0 0.5 all-gather.16.cloned.1.call-update
  10.5 0.7 all-gather.24.cloned.1.call-update
  11.3 0.7 all-gather.26.cloned.1.call-update
  12.1 0.1 fusion.9
  12.3 0.5 copy-done.2
  12.9 8.7 %all_gather.37 = bf16[128,2048]{1,0:T(8,128)(2,1)S(1)} all-gather(bf16[32,2048]{1,0:T(8,128)(2,1)S(1)} %fusion.11), channel_id=1, replica_groups=mesh['sp'=8,'tp'=4] {'tp'}, dimensions={0}, use_global_device_ids=true | all-gather | bytes 655360 | tf_op jit(solution)/shard_map/all_gather | solution.py:148
  21.6 0.7 copy-done.7
  22.4 30.1 %all-gather.20.cloned.1.call-done = bf16[2048,256]{1,0:T(8,128)(2,1)} async-done(((bf16[256,256]{1,0:T(8,128)(2,1)}), bf16[2048,256]{1,0:T(8,128)(2,1)}) %all-gather.20.cloned.1.call-update) | async-done | bytes 1048592 | tf_op jit(solution)/shard_map/all_gather | solution.py:129
  52.5 1.7 exponential-minus-one_negate_fusion
  54.4 0.1 reduce_window_sum.22
  54.6 39.0 %all-gather.22.cloned.1.call-done = bf16[2048,256]{1,0:T(8,128)(2,1)} async-done(((bf16[256,256]{1,0:T(8,128)(2,1)}), bf16[2048,256]{1,0:T(8,128)(2,1)}) %all-gather.22.cloned.1.call-update) | async-done | bytes 1048592 | tf_op jit(solution)/shard_map/all_gather | solution.py:130
  93.6 1.5 convolution_convert_fusion.2
  95.2 0.4 fusion.24
  95.6 0.4 while.27
  96.0 32.5 %all-gather.1 = bf16[16,128,128]{2,1,0:T(8,128)(2,1)S(1)} all-gather(bf16[2,128,128]{2,1,0:T(8,128)(2,1)S(1)} %convert_element_type.128), channel_id=3, replica_groups=mesh['sp'=8,'tp'=4] {'sp'}, dimensions={0}, use_global_device_ids=true | all-gather | bytes 589824 | tf_op jit(solution)/shard_map/all_gather | solution.py:24
  128.5 17.8 %all-gather.2 = bf16[8,2,128]{2,1,0:T(2,128)(2,1)S(1)} all-gather(bf16[1,2,128]{2,1,0:T(2,128)(2,1)S(1)} %bitcast.113), channel_id=2, replica_groups=mesh['sp'=8,'tp'=4] {'sp'}, dimensions={0}, use_global_device_ids=true | all-gather | bytes 4608 | tf_op jit(solution)/shard_map/all_gather | solution.py:24
  146.3 1.4 while.28
  146.3 0.1 fusion.69
  146.5 0.1 fusion.69
  146.7 0.1 fusion.69
  146.9 0.1 fusion.69
  147.2 0.1 fusion.69
  147.7 1.6 divide_multiply_fusion.1
  149.4 28.2 %all-gather.12.cloned.1.call-done = bf16[2048,256]{1,0:T(8,128)(2,1)} async-done(((bf16[256,256]{1,0:T(8,128)(2,1)}), bf16[2048,256]{1,0:T(8,128)(2,1)}) %all-gather.12.cloned.1.call-update) | async-done | bytes 1048592 | tf_op jit(solution)/shard_map/all_gather | solution.py:126
  177.6 1.5 convolution_convert_fusion.6
  179.1 2.5 collective-permute-start
  181.6 36.9 %all-gather.14.cloned.1.call-done = bf16[2048,256]{1,0:T(8,128)(2,1)} async-done(((bf16[256,256]{1,0:T(8,128)(2,1)}), bf16[2048,256]{1,0:T(8,128)(2,1)}) %all-gather.14.cloned.1.call-update) | async-done | bytes 1048592 | tf_op jit(solution)/shard_map/all_gather | solution.py:127
  218.6 1.5 convolution_convert_fusion.5
  220.1 2.5 collective-permute-start.1
  222.6 0.4 convolution_select_fusion
  223.0 0.2 fusion.36
  223.2 0.5 multiply_reduce_fusion
  224.2 2.2 fusion.51
  226.4 5.7 %all-reduce = (f32[128]{0:T(128)S(1)}, f32[128]{0:T(128)S(1)}) all-reduce(f32[128]{0:T(128)S(1)} %fusion.23, f32[128]{0:T(128)S(1)} %get-tuple-element.194), channel_id=1, replica_groups=mesh['sp'=8,'tp'=4] {'tp'}, use_global_device_ids=true, to_apply=%region_4.5 | all-reduce | flops 256 | bytes 2048 | tf_op jit(solution)/shard_map/psum | solution.py:212
  232.1 26.5 %all-gather.16.cloned.1.call-done = bf16[256,2048]{1,0:T(8,128)(2,1)} async-done(((bf16[256,256]{1,0:T(8,128)(2,1)}), bf16[256,2048]{1,0:T(8,128)(2,1)}) %all-gather.16.cloned.1.call-update) | async-done | bytes 1048592 | tf_op jit(solution)/shard_map/all_gather | solution.py:132
  258.7 0.7 copy-done.3
  259.3 1.6 fusion.34
  261.0 39.2 %all-gather.24.cloned.1.call-done = bf16[2048,256]{1,0:T(8,128)(2,1)} async-done(((bf16[256,256]{1,0:T(8,128)(2,1)}), bf16[2048,256]{1,0:T(8,128)(2,1)}) %all-gather.24.cloned.1.call-update) | async-done | bytes 1048592 | tf_op jit(solution)/shard_map/all_gather | solution.py:131
  300.1 40.2 %all-gather.26.cloned.1.call-done = bf16[256,2048]{1,0:T(8,128)(2,1)} async-done(((bf16[256,256]{1,0:T(8,128)(2,1)}), bf16[256,2048]{1,0:T(8,128)(2,1)}) %all-gather.26.cloned.1.call-update) | async-done | bytes 1048592 | tf_op jit(solution)/shard_map/all_gather | solution.py:133
  340.3 0.2 mul.161
  340.5 0.7 copy-done.5
  341.2 3.1 fusion.1
  344.3 20.9 %reduce-scatter.2.cloned.1.call-done = bf16[32,2048]{1,0:T(8,128)(2,1)} async-done(((bf16[128,2048]{1,0:T(8,128)(2,1)}), bf16[32,2048]{1,0:T(8,128)(2,1)}) %reduce-scatter.2.cloned.1.call-update) | async-done | bytes 131088 | tf_op jit(solution)/shard_map/reduce_scatter | solution.py:217
  (67 shorter events, 2.2 us)
Async XLA Ops:
  6.5 217.6 %copy-start = (f32[31,256]{1,0:T(8,128)S(1)}, f32[31,256]{1,0:T(8,128)}, u32[]{:S(2)}) copy-start(f32[31,256]{1,0:T(8,128)} %param.24) | copy-start | bytes 95236
  6.5 46.0 %all-gather.20.cloned.1.call-start = ((), (), s32[]{:S(2)}) async-start(), calls=%async_computation.5 | async-start | bytes 1179648 | tf_op jit(solution)/shard_map/all_gather | solution.py:129
  7.3 86.4 %all-gather.22.cloned.1.call-start = ((), (), s32[]{:S(2)}) async-start(), calls=%async_computation.6 | async-start | bytes 1179648 | tf_op jit(solution)/shard_map/all_gather | solution.py:130
  8.0 139.7 %all-gather.18.cloned.1.call-start = ((), (), s32[]{:S(2)}) async-start(), calls=%async_computation.4 | async-start | bytes 1179648 | tf_op jit(solution)/shard_map/all_gather | solution.py:128
  8.7 168.8 %all-gather.12.cloned.1.call-start = ((), (), s32[]{:S(2)}) async-start(), calls=%async_computation.1 | async-start | bytes 1179648 | tf_op jit(solution)/shard_map/all_gather | solution.py:126
  9.3 209.3 %all-gather.14.cloned.1.call-start = ((), (), s32[]{:S(2)}) async-start(), calls=%async_computation.2 | async-start | bytes 1179648 | tf_op jit(solution)/shard_map/all_gather | solution.py:127
  9.9 248.8 %all-gather.16.cloned.1.call-start = ((), (), s32[]{:S(2)}) async-start(), calls=%async_computation.3 | async-start | bytes 1179648 | tf_op jit(solution)/shard_map/all_gather | solution.py:132
  10.5 1.6 copy-start.1
  10.5 289.6 %all-gather.24.cloned.1.call-start = ((), (), s32[]{:S(2)}) async-start(), calls=%async_computation.7 | async-start | bytes 1179648 | tf_op jit(solution)/shard_map/all_gather | solution.py:131
  11.2 329.1 %all-gather.26.cloned.1.call-start = ((), (), s32[]{:S(2)}) async-start(), calls=%async_computation.8 | async-start | bytes 1179648 | tf_op jit(solution)/shard_map/all_gather | solution.py:133
  12.0 353.2 %reduce-scatter.2.cloned.1.call-start = ((), (), s32[]{:S(2)}) async-start(), calls=%async_computation.9 | async-start | bytes 655360 | tf_op jit(solution)/shard_map/reduce_scatter | solution.py:217
  12.1 0.7 copy-start.2
  12.9 8.7 %copy-start.6 = (f32[256]{0:T(256)S(1)}, f32[256]{0:T(256)}, u32[]{:S(2)}) copy-start(f32[256]{0:T(256)} %param.31) | copy-start | bytes 3076
  21.6 0.7 copy-start.7
  179.1 44.9 %collective-permute-start = (bf16[30,256]{1,0:T(8,128)(2,1)S(1)}, bf16[30,256]{1,0:T(8,128)(2,1)S(1)}, u32[]{:S(2)}, u32[]{:S(2)}) collective-permute-start(bf16[30,256]{1,0:T(8,128)(2,1)S(1)} %slice.12), channel_id=1, source_target_pairs={{0,4},{4,8},{8,12},{12,16},{16,20},{20,24},{24,28},{1,5},{5,9},{9,... | collective-permute-start | bytes 46088 | tf_op jit(solution)/shard_map/ppermute | solution.py:18
  220.1 3.9 %collective-permute-start.1 = (bf16[30,256]{1,0:T(8,128)(2,1)S(1)}, bf16[30,256]{1,0:T(8,128)(2,1)S(1)}, u32[]{:S(2)}, u32[]{:S(2)}) collective-permute-start(bf16[30,256]{1,0:T(8,128)(2,1)S(1)} %slice.13), channel_id=1, source_target_pairs={{0,4},{4,8},{8,12},{12,16},{16,20},{20,24},{24,28},{1,5},{5,9},{9,... | collective-permute-start | bytes 46088 | tf_op jit(solution)/shard_map/ppermute | solution.py:18
  224.1 34.5 %copy-start.4 = (f32[256]{0:T(256)S(1)}, f32[256]{0:T(256)}, u32[]{:S(2)}) copy-start(f32[256]{0:T(256)} %param.25) | copy-start | bytes 3076
  258.7 0.7 copy-start.3
  340.5 0.7 copy-start.5
Sparse Core Ops, SparseCore 0:
  9.5 42.9 all-gather.19
  54.6 38.9 all-gather.21
  95.8 40.5 all-gather.17
  138.4 39.1 all-gather.11
  179.6 38.9 all-gather.13
  220.5 38.1 all-gather.15
  260.8 39.2 all-gather.23
  302.2 38.0 all-gather.25
  344.5 20.6 reduce-scatter.1
where the time goes:
time: 372 us
  waiting for transfers between devices  266 us (72%)
  blocking collectives  64.7 us (17%)
  matrix products  16.3 us (4%)
  between operations  13.5 us (4%)
  starting transfers between devices  5.28 us (1%)
    all_gather x2, blocking collectives, prefix(): lax.all_gather(part.astype(kind), axis)  50.3 us
    all_gather x1, waiting for transfers between devices, per_device(): lax.all_gather(recurrence_output_weight, 'sp', axis=1, tiled=True)  40.2 us
    all_gather x1, waiting for transfers between devices, per_device(): lax.all_gather(output_gate_weight, 'sp', axis=0, tiled=True)  39.2 us
    all_gather x1, waiting for transfers between devices, per_device(): lax.all_gather(recurrence_value_weight, 'sp', axis=0, tiled=True)  39 us
    all_gather x1, waiting for transfers between devices, per_device(): lax.all_gather(convolution_gate_weight, 'sp', axis=0, tiled=True)  36.9 us
    all_gather x1, waiting for transfers between devices, per_device(): lax.all_gather(forget_gate_weight, 'sp', axis=0, tiled=True)  30.1 us
    all_gather x1, waiting for transfers between devices, per_device(): lax.all_gather(convolution_value_weight, 'sp', axis=0, tiled=True)  28.2 us
    all_gather x1, waiting for transfers between devices, per_device(): lax.all_gather(convolution_output_weight, 'sp', axis=1, tiled=True)  26.5 us
  transfers between devices with their start and end apart: 11, of which 8 were waited for; matrix products, arithmetic and copies ran while one was open for 4% of the time, Pallas kernels for 0%

commit v1 on v0

--- a/solution.py
+++ b/solution.py
@@ -10,6 +10,11 @@
 norm_eps = 1e-06
 layer_eps = 1e-05
 highest_precision = lax.Precision.HIGHEST
+
+
+def all_by_exchange(x, axis, dim):
+    sent = jnp.stack([x] * lax.axis_size(axis))
+    return jnp.concatenate(lax.all_to_all(sent, axis, 0, 0), axis=dim)
 
 
 def passed_along(value, axis, steps):
@@ -124,7 +129,7 @@
     ).astype(jnp.bfloat16)
     gathered = (
         lax.all_gather(convolution_value_weight, "sp", axis=0, tiled=True),
-        lax.all_gather(convolution_gate_weight, "sp", axis=0, tiled=True),
+        all_by_exchange(convolution_gate_weight, "sp", 0),
         lax.all_gather(query_projection_weight, "sp", axis=0, tiled=True),
         lax.all_gather(forget_gate_weight, "sp", axis=0, tiled=True),
         lax.all_gather(recurrence_value_weight, "sp", axis=0, tiled=True),

time: 372 us -> 339 us (0.911)
  waiting for transfers between devices: 266 us -> 227 us
  starting transfers between devices: 5.28 us -> 12.6 us
    all_gather x1 -> x0, waiting for transfers between devices: 36.9 us -> none  [per_device(): lax.all_gather(convolution_gate_weight, 'sp', axis=0, tiled=True)]
    all_to_all x0 -> x1, starting transfers between devices: none -> 7.28 us  [all_by_exchange(): return jnp.concatenate(lax.all_to_all(sent, axis, 0, 0), axis=dim)]
  transfers between devices with their start and end apart: 11 -> 11, of which waited for: 8 -> 8; matrix products, arithmetic and copies ran while one was open for 4% -> 5% of each run, Pallas kernels for 0% -> 0%
where the time goes in v1:
time: 339 us
  waiting for transfers between devices  227 us (67%)
  blocking collectives  63.1 us (19%)
  matrix products  15.1 us (4%)
  between operations  13.8 us (4%)
  starting transfers between devices  12.6 us (4%)
  local copies, waits for them, and re-layouts  4.45 us (1%)
    all_gather x2, blocking collectives, prefix(): lax.all_gather(part.astype(kind), axis)  50.2 us
    all_gather x1, waiting for transfers between devices, per_device(): lax.all_gather(recurrence_output_weight, 'sp', axis=1, tiled=True)  40.2 us
    all_gather x1, waiting for transfers between devices, per_device(): lax.all_gather(recurrence_value_weight, 'sp', axis=0, tiled=True)  39.1 us
    all_gather x1, waiting for transfers between devices, per_device(): lax.all_gather(output_gate_weight, 'sp', axis=0, tiled=True)  39 us
    all_gather x1, waiting for transfers between devices, per_device(): lax.all_gather(forget_gate_weight, 'sp', axis=0, tiled=True)  31.8 us
    all_gather x1, waiting for transfers between devices, per_device(): lax.all_gather(convolution_output_weight, 'sp', axis=1, tiled=True)  26.5 us
    all_gather x1, waiting for transfers between devices, per_device(): lax.all_gather(convolution_value_weight, 'sp', axis=0, tiled=True)  25.5 us
    reduce_scatter x1, waiting for transfers between devices, per_device(): lax.psum_scatter((jnp.dot(conv_part, conv_columns, preferred_element_type...  20.9 us
  transfers between devices with their start and end apart: 11, of which 8 were waited for; matrix products, arithmetic and copies ran while one was open for 5% of the time, Pallas kernels for 0%

profile of v1, /device:TPU:0, one launch (start us, length us, event | category | flops | bytes accessed | tf_op | source)
XLA Modules:
  0.0 338.8 jit_solution(12769308794320723816)
XLA Ops:
  6.5 0.7 all-gather.17.cloned.1.call-update
  7.3 0.7 all-gather.19.cloned.1.call-update
  8.1 0.7 all-gather.15.cloned.1.call-update
  8.8 0.5 all-gather.11.cloned.1.call-update
  9.4 0.5 all-gather.13.cloned.1.call-update
  10.0 0.5 all-gather.21.cloned.1.call-update
  10.5 1.0 stack.2
  11.5 7.3 %all-to-all-start = ((bf16[8,256,256]{2,1,0:T(8,128)(2,1)}), bf16[8,256,256]{2,1,0:T(8,128)(2,1)S(1)}, u32[]{:S(2)}, u32[]{:S(2)}) async-start(bf16[8,256,256]{2,1,0:T(8,128)(2,1)} %stack.2), calls=%async_computation | async-start | bytes 2097152 | tf_op jit(solution)/shard_map/all_to_all | solution.py:17
  18.9 0.7 all-gather.23.cloned.1.call-update
  19.7 0.1 fusion.9
  19.9 0.5 copy-done.3
  20.5 7.2 %all_gather.34 = bf16[128,2048]{1,0:T(8,128)(2,1)S(1)} all-gather(bf16[32,2048]{1,0:T(8,128)(2,1)S(1)} %fusion.11), channel_id=1, replica_groups=mesh['sp'=8,'tp'=4] {'tp'}, dimensions={0}, use_global_device_ids=true | all-gather | bytes 655360 | tf_op jit(solution)/shard_map/all_gather | solution.py:153
  27.8 0.7 copy-done.8
  28.5 31.8 %all-gather.17.cloned.1.call-done = bf16[2048,256]{1,0:T(8,128)(2,1)} async-done(((bf16[256,256]{1,0:T(8,128)(2,1)}), bf16[2048,256]{1,0:T(8,128)(2,1)}) %all-gather.17.cloned.1.call-update) | async-done | bytes 1048592 | tf_op jit(solution)/shard_map/all_gather | solution.py:134
  60.4 1.7 exponential-minus-one_negate_fusion
  62.3 0.1 reduce_window_sum.22
  62.5 39.1 %all-gather.19.cloned.1.call-done = bf16[2048,256]{1,0:T(8,128)(2,1)} async-done(((bf16[256,256]{1,0:T(8,128)(2,1)}), bf16[2048,256]{1,0:T(8,128)(2,1)}) %all-gather.19.cloned.1.call-update) | async-done | bytes 1048592 | tf_op jit(solution)/shard_map/all_gather | solution.py:135
  101.6 1.5 convolution_convert_fusion.2
  103.1 0.4 fusion.24
  103.5 0.4 while.27
  103.9 32.5 %all-gather.1 = bf16[16,128,128]{2,1,0:T(8,128)(2,1)S(1)} all-gather(bf16[2,128,128]{2,1,0:T(8,128)(2,1)S(1)} %convert_element_type.128), channel_id=3, replica_groups=mesh['sp'=8,'tp'=4] {'sp'}, dimensions={0}, use_global_device_ids=true | all-gather | bytes 589824 | tf_op jit(solution)/shard_map/all_gather | solution.py:29
  136.4 17.7 %all-gather.2 = bf16[8,2,128]{2,1,0:T(2,128)(2,1)S(1)} all-gather(bf16[1,2,128]{2,1,0:T(2,128)(2,1)S(1)} %bitcast.115), channel_id=2, replica_groups=mesh['sp'=8,'tp'=4] {'sp'}, dimensions={0}, use_global_device_ids=true | all-gather | bytes 4608 | tf_op jit(solution)/shard_map/all_gather | solution.py:29
  154.1 1.5 divide_multiply_fusion.1
  155.8 1.4 while.28
  155.8 0.1 fusion.69
  156.0 0.1 fusion.69
  156.1 0.1 fusion.69
  156.3 0.1 fusion.69
  156.5 0.1 fusion.69
  157.2 0.3 convolution_convert_fusion.5
  157.5 2.5 collective-permute-start.1
  160.0 25.5 %all-gather.11.cloned.1.call-done = bf16[2048,256]{1,0:T(8,128)(2,1)} async-done(((bf16[256,256]{1,0:T(8,128)(2,1)}), bf16[2048,256]{1,0:T(8,128)(2,1)}) %all-gather.11.cloned.1.call-update) | async-done | bytes 1048592 | tf_op jit(solution)/shard_map/all_gather | solution.py:131
  185.6 1.5 convolution_convert_fusion.6
  187.1 2.5 collective-permute-start
  189.6 0.4 convolution_select_fusion
  190.0 0.2 fusion.36
  190.2 0.5 multiply_reduce_fusion
  191.1 2.2 fusion.51
  193.4 5.7 %all-reduce = (f32[128]{0:T(128)S(1)}, f32[128]{0:T(128)S(1)}) all-reduce(f32[128]{0:T(128)S(1)} %fusion.23, f32[128]{0:T(128)S(1)} %get-tuple-element.194), channel_id=1, replica_groups=mesh['sp'=8,'tp'=4] {'tp'}, use_global_device_ids=true, to_apply=%region_4.5 | all-reduce | flops 256 | bytes 2048 | tf_op jit(solution)/shard_map/psum | solution.py:217
  199.1 26.5 %all-gather.13.cloned.1.call-done = bf16[256,2048]{1,0:T(8,128)(2,1)} async-done(((bf16[256,256]{1,0:T(8,128)(2,1)}), bf16[256,2048]{1,0:T(8,128)(2,1)}) %all-gather.13.cloned.1.call-update) | async-done | bytes 1048592 | tf_op jit(solution)/shard_map/all_gather | solution.py:137
  225.6 0.7 copy-done.4
  226.3 1.6 fusion.34
  227.9 39.0 %all-gather.21.cloned.1.call-done = bf16[2048,256]{1,0:T(8,128)(2,1)} async-done(((bf16[256,256]{1,0:T(8,128)(2,1)}), bf16[2048,256]{1,0:T(8,128)(2,1)}) %all-gather.21.cloned.1.call-update) | async-done | bytes 1048592 | tf_op jit(solution)/shard_map/all_gather | solution.py:136
  266.9 40.2 %all-gather.23.cloned.1.call-done = bf16[256,2048]{1,0:T(8,128)(2,1)} async-done(((bf16[256,256]{1,0:T(8,128)(2,1)}), bf16[256,2048]{1,0:T(8,128)(2,1)}) %all-gather.23.cloned.1.call-update) | async-done | bytes 1048592 | tf_op jit(solution)/shard_map/all_gather | solution.py:138
  307.1 0.2 mul.161
  307.3 0.7 copy-done.6
  308.0 3.2 fusion.1
  311.1 20.9 %reduce-scatter.2.cloned.1.call-done = bf16[32,2048]{1,0:T(8,128)(2,1)} async-done(((bf16[128,2048]{1,0:T(8,128)(2,1)}), bf16[32,2048]{1,0:T(8,128)(2,1)}) %reduce-scatter.2.cloned.1.call-update) | async-done | bytes 131088 | tf_op jit(solution)/shard_map/reduce_scatter | solution.py:222
  (69 shorter events, 2.2 us)
Async XLA Ops:
  6.5 184.6 %copy-start = (f32[31,256]{1,0:T(8,128)S(1)}, f32[31,256]{1,0:T(8,128)}, u32[]{:S(2)}) copy-start(f32[31,256]{1,0:T(8,128)} %param.24) | copy-start | bytes 95236
  6.5 53.8 %all-gather.17.cloned.1.call-start = ((), (), s32[]{:S(2)}) async-start(), calls=%async_computation.5 | async-start | bytes 1179648 | tf_op jit(solution)/shard_map/all_gather | solution.py:134
  7.3 94.3 %all-gather.19.cloned.1.call-start = ((), (), s32[]{:S(2)}) async-start(), calls=%async_computation.6 | async-start | bytes 1179648 | tf_op jit(solution)/shard_map/all_gather | solution.py:135
  8.0 146.1 %all-gather.15.cloned.1.call-start = ((), (), s32[]{:S(2)}) async-start(), calls=%async_computation.4 | async-start | bytes 1179648 | tf_op jit(solution)/shard_map/all_gather | solution.py:133
  8.7 176.8 %all-gather.11.cloned.1.call-start = ((), (), s32[]{:S(2)}) async-start(), calls=%async_computation.2 | async-start | bytes 1179648 | tf_op jit(solution)/shard_map/all_gather | solution.py:131
  9.3 1.2 copy-start.2
  9.3 216.3 %all-gather.13.cloned.1.call-start = ((), (), s32[]{:S(2)}) async-start(), calls=%async_computation.3 | async-start | bytes 1179648 | tf_op jit(solution)/shard_map/all_gather | solution.py:137
  9.9 257.0 %all-gather.21.cloned.1.call-start = ((), (), s32[]{:S(2)}) async-start(), calls=%async_computation.7 | async-start | bytes 1179648 | tf_op jit(solution)/shard_map/all_gather | solution.py:136
  11.5 145.6 %all-to-all-start = ((bf16[8,256,256]{2,1,0:T(8,128)(2,1)}), bf16[8,256,256]{2,1,0:T(8,128)(2,1)S(1)}, u32[]{:S(2)}, u32[]{:S(2)}) async-start(bf16[8,256,256]{2,1,0:T(8,128)(2,1)} %stack.2), calls=%async_computation | async-start | bytes 2097152 | tf_op jit(solution)/shard_map/all_to_all | solution.py:17
  18.8 0.9 copy-start.1
  18.8 288.3 %all-gather.23.cloned.1.call-start = ((), (), s32[]{:S(2)}) async-start(), calls=%async_computation.8 | async-start | bytes 1179648 | tf_op jit(solution)/shard_map/all_gather | solution.py:138
  19.6 312.4 %reduce-scatter.2.cloned.1.call-start = ((), (), s32[]{:S(2)}) async-start(), calls=%async_computation.9 | async-start | bytes 655360 | tf_op jit(solution)/shard_map/reduce_scatter | solution.py:222
  19.7 0.7 copy-start.3
  20.5 7.2 %copy-start.7 = (f32[256]{0:T(256)S(1)}, f32[256]{0:T(256)}, u32[]{:S(2)}) copy-start(f32[256]{0:T(256)} %param.31) | copy-start | bytes 3076
  27.8 0.7 copy-start.8
  157.5 33.5 %collective-permute-start.1 = (bf16[30,256]{1,0:T(8,128)(2,1)S(1)}, bf16[30,256]{1,0:T(8,128)(2,1)S(1)}, u32[]{:S(2)}, u32[]{:S(2)}) collective-permute-start(bf16[30,256]{1,0:T(8,128)(2,1)S(1)} %slice.13), channel_id=1, source_target_pairs={{0,4},{4,8},{8,12},{12,16},{16,20},{20,24},{24,28},{1,5},{5,9},{9,... | collective-permute-start | bytes 46088 | tf_op jit(solution)/shard_map/ppermute | solution.py:23
  187.1 3.9 %collective-permute-start = (bf16[30,256]{1,0:T(8,128)(2,1)S(1)}, bf16[30,256]{1,0:T(8,128)(2,1)S(1)}, u32[]{:S(2)}, u32[]{:S(2)}) collective-permute-start(bf16[30,256]{1,0:T(8,128)(2,1)S(1)} %slice.12), channel_id=1, source_target_pairs={{0,4},{4,8},{8,12},{12,16},{16,20},{20,24},{24,28},{1,5},{5,9},{9,... | collective-permute-start | bytes 46088 | tf_op jit(solution)/shard_map/ppermute | solution.py:23
  191.1 34.5 %copy-start.5 = (f32[256]{0:T(256)S(1)}, f32[256]{0:T(256)}, u32[]{:S(2)}) copy-start(f32[256]{0:T(256)} %param.25) | copy-start | bytes 3076
  225.6 0.7 copy-start.4
  307.3 0.7 copy-start.6
Sparse Core Ops, SparseCore 0:
  9.5 50.8 all-gather.16
  62.5 39.0 all-gather.18
  103.7 40.5 all-gather.14
  146.3 39.2 all-gather.10
  187.5 38.0 all-gather.12
  227.6 39.2 all-gather.20
  268.9 38.0 all-gather.22
  311.3 20.6 reduce-scatter.1
